TPU v7x, 32 devices: a whole 2x2x4 slice. The times are simulated.
32 devices in a mesh: grp: 2 (over x), ep: 16 (over z, y, core).
Axes of the slice: x: 2, y: 2, z: 4, core: 2. Of those that a mesh axis runs over, the one named last changes fastest.
Arguments:
- hidden: bfloat16 [96, 2048], P(('grp', 'ep')), parts along dimension 0, may hold values from -6 to 6
- conv_window: bfloat16 [96, 3, 6144], P(('grp', 'ep')), parts along dimension 0, may hold values from -6 to 6
- ssm_state: float32 [96, 64, 64, 128], P(('grp', 'ep')), parts along dimension 0, may hold values from -1.75 to 1.75
- gate_proj: bfloat16 [2048, 4096], P(None, 'ep'), may hold values from -0.125 to 0.125
- input_proj: bfloat16 [2048, 4096], P(None, 'ep'), may hold values from -0.125 to 0.125
- write_proj: bfloat16 [2048, 1024], P(None, 'ep'), may hold values from -0.125 to 0.125
- read_proj: bfloat16 [2048, 1024], P(None, 'ep'), may hold values from -0.125 to 0.125
- step_proj: bfloat16 [2048, 64], replicated, may hold values from -0.125 to 0.125
- step_bias: float32 [64], replicated, may hold values from -2 to 1
- decay_log: float32 [64], replicated, may hold values from -2.3 to 1.4
- decay_shift: float32 [96, 64], P(('grp', 'ep')), parts along dimension 0, may hold values from -0.7 to 0
- skip_scale: float32 [64], replicated, may hold values from -4 to 4
- conv_taps: bfloat16 [4, 6144], replicated, may hold values from -3 to 3
- conv_bias: float32 [6144], replicated, may hold values from -3 to 3
- mix_gain: float32 [2048], replicated, may hold values from 0.1 to 1.9
- group_gain: float32 [4096], replicated, may hold values from 0.1 to 1.9
- out_proj: bfloat16 [4096, 2048], P(None, 'ep'), may hold values from -0.09375 to 0.09375
- ffn_gain: float32 [2048], replicated, may hold values from 0.1 to 1.9
- router: bfloat16 [2048, 16], replicated, may hold values from -0.125 to 0.125
- expert_ids: int32 [96, 6], P(('grp', 'ep')), parts along dimension 0, may hold values from 0 to 15, all different within a row; in each aligned block of 3 rows (0 to 2, 3 to 5, ...) at most 2 rows name the same one
- expert_gate: bfloat16 [16, 2048, 512], P('ep'), may hold values from -0.125 to 0.125
- expert_up: bfloat16 [16, 2048, 512], P('ep'), may hold values from -0.125 to 0.125
- expert_down: bfloat16 [16, 512, 2048], P('ep'), may hold values from -0.25 to 0.25
- shared_gate: bfloat16 [2048, 512], P('ep'), may hold values from -0.125 to 0.125
- shared_up: bfloat16 [2048, 512], P('ep'), may hold values from -0.125 to 0.125
- shared_down: bfloat16 [512, 2048], replicated, may hold values from -0.25 to 0.25
Outputs:
- layer_out: bfloat16 [96, 2048], P(('grp', 'ep')), parts along dimension 0
- next_state: float32 [96, 64, 64, 128], P(('grp', 'ep')), parts along dimension 0
- next_window: bfloat16 [96, 3, 6144], P(('grp', 'ep')), parts along dimension 0
There are 2 independent parts, one for each index of `grp`. A program takes and returns all parts, laid end to end along the dimension named above; an argument that names none is the same for every part. Nothing has to cross between parts.
Inputs may be any that keep to these rules, and one draw needn't show every extreme that they name: `expert_ids`: each row names 6 different experts; in the rows of one device no expert is named by more than 2 rows, and in every draw some device's rows name some expert exactly 2 times.
All inputs are finite; a program needn't handle non-finite values.
Results may differ from a plain program's by a relative error of at most 0.019.
Values may be sent and summed in bfloat16 or wider, within the bound.
A program may use at most 128 MiB of HBM per device.

v0:
```python
import jax
import jax.numpy as jnp
from jax import lax
from jax.sharding import PartitionSpec as P

HEAD_DIM = 64
GROUPS = 8
STATE = 128
CAP = 2


epsilon = 1e-06
routed_scale = 2.5


def row_scale(values):
    return lax.rsqrt(jnp.mean(values * values, axis=-1, keepdims=True) + epsilon)


def matmul(left, right):
    return jnp.dot(left, right, preferred_element_type=jnp.float32)


def expert_result(rows_in, weight_gate, weight_up, weight_down):
    expert_hidden = (jax.nn.silu(matmul(rows_in, weight_gate)) * matmul(rows_in, weight_up)).astype(
        jnp.bfloat16
    )
    return matmul(expert_hidden, weight_down).astype(jnp.bfloat16)


def route_weights(routed_in, router, chosen):
    scores = jax.nn.sigmoid(matmul(routed_in, router))
    picked = jnp.take_along_axis(scores, chosen, axis=1)
    return routed_scale * picked / jnp.sum(picked, axis=1, keepdims=True)


def shards(
    hidden,
    conv_window,
    ssm_state,
    gate_proj,
    input_proj,
    write_proj,
    read_proj,
    step_proj,
    step_bias,
    decay_log,
    decay_shift,
    skip_scale,
    conv_taps,
    conv_bias,
    mix_gain,
    group_gain,
    out_proj,
    ffn_gain,
    router,
    expert_ids,
    expert_gate,
    expert_up,
    expert_down,
    shared_gate,
    shared_up,
    shared_down,
):
    local_rows = hidden.shape[0]
    device_index = lax.axis_index("ep")
    gathered = lax.all_gather(hidden, "ep", axis=0, tiled=True)
    gathered_wide = gathered.astype(jnp.float32)
    normed = (gathered_wide * row_scale(gathered_wide) * mix_gain).astype(jnp.bfloat16)
    gate_part = matmul(normed, gate_proj).astype(jnp.bfloat16)
    input_part = matmul(normed, input_proj).astype(jnp.bfloat16)
    write_part = matmul(normed, write_proj).astype(jnp.bfloat16)
    read_part = matmul(normed, read_proj).astype(jnp.bfloat16)
    gate_rows, input_rows, write_rows, read_rows = (
        lax.all_to_all(gate_part, "ep", split_axis=0, concat_axis=1, tiled=True),
        lax.all_to_all(input_part, "ep", split_axis=0, concat_axis=1, tiled=True),
        lax.all_to_all(write_part, "ep", split_axis=0, concat_axis=1, tiled=True),
        lax.all_to_all(read_part, "ep", split_axis=0, concat_axis=1, tiled=True),
    )
    normed_local = lax.dynamic_slice_in_dim(normed, device_index * local_rows, local_rows, 0)
    step_raw = matmul(normed_local, step_proj)
    inner_width = gate_rows.shape[1]
    state_span = GROUPS * STATE
    head_count = step_bias.shape[0]
    per_group = head_count // GROUPS
    fresh_row = jnp.concatenate([input_rows, write_rows, read_rows], axis=1)
    window = jnp.concatenate([conv_window, fresh_row[:, None, :]], axis=1)
    convolved = jax.nn.silu(
        jnp.sum(window.astype(jnp.float32) * conv_taps.astype(jnp.float32)[None], axis=1)
        + conv_bias
    )
    head_input = convolved[:, :inner_width].reshape(local_rows, GROUPS, per_group, HEAD_DIM)
    write_vec = convolved[:, inner_width : inner_width + state_span].reshape(
        local_rows, GROUPS, STATE
    )
    read_vec = convolved[:, inner_width + state_span :].reshape(local_rows, GROUPS, STATE)
    step_size = jax.nn.softplus(step_raw + step_bias)
    decay_rate = jnp.exp(decay_shift - step_size * jnp.exp(decay_log)).reshape(
        local_rows, GROUPS, per_group
    )
    step_group = step_size.reshape(local_rows, GROUPS, per_group)
    carried = ssm_state.reshape(local_rows, GROUPS, per_group, HEAD_DIM, STATE)
    next_state = (
        decay_rate[..., None, None] * carried
        + (step_group[..., None] * head_input)[..., None] * write_vec[:, :, None, None, :]
    )
    mixed_out = jnp.einsum("sgepn,sgn->sgep", next_state, read_vec, precision=lax.Precision.HIGHEST)
    mixed_out = mixed_out + skip_scale.reshape(GROUPS, per_group)[None, :, :, None] * head_input
    mixed_out = mixed_out.reshape(local_rows, inner_width).astype(jnp.bfloat16)
    gated_out = mixed_out.astype(jnp.float32) * jax.nn.silu(gate_rows.astype(jnp.float32))
    blocks = gated_out.reshape(local_rows, GROUPS, -1)
    gated_out = ((blocks * row_scale(blocks)).reshape(local_rows, inner_width) * group_gain).astype(
        jnp.bfloat16
    )
    col_width = out_proj.shape[1]
    resid_cols = lax.dynamic_slice_in_dim(gathered_wide, device_index * col_width, col_width, 1)
    resid_part = (
        resid_cols + matmul(lax.all_gather(gated_out, "ep", axis=0, tiled=True), out_proj)
    ).astype(jnp.bfloat16)
    gain_part = lax.dynamic_slice_in_dim(ffn_gain, device_index * col_width, col_width, 0)
    shared_part = (resid_part.astype(jnp.float32) * gain_part).astype(jnp.bfloat16)
    shared_pre = lax.psum_scatter(
        jnp.concatenate(
            [matmul(shared_part, shared_gate), matmul(shared_part, shared_up)], axis=1
        ).astype(jnp.bfloat16),
        "ep",
        scatter_dimension=0,
        tiled=True,
    ).astype(jnp.float32)
    exp_dev = expert_gate.shape[0]
    resid = lax.all_to_all(resid_part, "ep", split_axis=0, concat_axis=1, tiled=True)
    resid_wide = resid.astype(jnp.float32)
    norm_scale = row_scale(resid_wide)
    routed_in = (resid_wide * norm_scale * ffn_gain).astype(jnp.bfloat16)
    weights = route_weights(routed_in, router, expert_ids)
    expert_total = router.shape[1]
    member = jnp.any(
        expert_ids[:, :, None] == jnp.arange(expert_total, dtype=jnp.int32)[None, None, :], axis=1
    ).astype(jnp.int32)
    earlier = jnp.cumsum(member, axis=0) - member
    slot_index = jnp.take_along_axis(earlier, expert_ids, axis=1)
    places = expert_ids * CAP + slot_index
    dispatch_table = jnp.any(
        places[None, :, :] == jnp.arange(expert_total * CAP, dtype=jnp.int32)[:, None, None], axis=2
    ).astype(jnp.bfloat16)
    outbound = (
        matmul(dispatch_table, routed_in)
        .astype(jnp.bfloat16)
        .reshape(lax.axis_size("ep"), exp_dev, CAP, routed_in.shape[1])
    )
    arrived = lax.all_to_all(outbound, "ep", split_axis=0, concat_axis=0, tiled=True)
    rows_in = arrived[:, 0].reshape(-1, arrived.shape[-1])
    result = expert_result(rows_in, expert_gate[0], expert_up[0], expert_down[0])
    results = [result.reshape(arrived.shape[0], arrived.shape[2], arrived.shape[3])]
    returned = lax.all_to_all(
        jnp.stack(results, axis=1), "ep", split_axis=0, concat_axis=0, tiled=True
    )
    returned_flat = returned.reshape(expert_total * CAP, returned.shape[-1])
    picked = jnp.take(returned_flat, places.reshape(-1), axis=0).reshape(
        local_rows, expert_ids.shape[1], returned.shape[-1]
    )
    routed = jnp.sum(picked.astype(jnp.float32) * weights[:, :, None], axis=1)
    hidden_units = shared_down.shape[0]
    shared_hidden = (
        jax.nn.silu(norm_scale * shared_pre[:, :hidden_units])
        * (norm_scale * shared_pre[:, hidden_units:])
    ).astype(jnp.bfloat16)
    layer_out = (resid_wide + routed + matmul(shared_hidden, shared_down)).astype(jnp.bfloat16)
    return (layer_out, next_state.reshape(ssm_state.shape), window[:, 1:])


def solution(mesh):
    placed = (
        P(("grp", "ep"), None),
        P(("grp", "ep"), None, None),
        P(("grp", "ep"), None, None, None),
        P(None, "ep"),
        P(None, "ep"),
        P(None, "ep"),
        P(None, "ep"),
        P(),
        P(),
        P(),
        P(("grp", "ep"), None),
        P(),
        P(),
        P(),
        P(),
        P(),
        P(None, "ep"),
        P(),
        P(),
        P(("grp", "ep"), None),
        P("ep", None, None),
        P("ep", None, None),
        P("ep", None, None),
        P("ep", None),
        P("ep", None),
        P(),
    )
    return jax.shard_map(
        shards,
        mesh=mesh,
        in_specs=placed,
        out_specs=(
            P(("grp", "ep"), None),
            P(("grp", "ep"), None, None, None),
            P(("grp", "ep"), None, None),
        ),
        check_vma=False,
    )
```

profile of v0, /device:TPU:0, one launch (start us, length us, event | category | flops | bytes accessed | tf_op | source)
XLA Modules:
  0.0 219.6 jit_solution(2211372966477305906)
XLA Ops:
  7.3 24.2 %all-gather = bf16[16,3,2048]{2,1,0:T(4,128)(2,1)S(1)} all-gather(bf16[1,3,2048]{2,1,0:T(4,128)(2,1)} %bitcast.106), channel_id=1, replica_groups=mesh['grp'=2,'ep'=16] {'ep'}, dimensions={0}, use_global_device_ids=true | all-gather | bytes 208896 | tf_op jit(solution)/shard_map/all_gather | solution.py:67
  32.6 1.2 convolution_convert_fusion.7
  34.4 3.5 %all-to-all-start.1 = ((bf16[16,3,64]{2,1,0:T(4,128)(2,1)}), bf16[16,3,64]{2,1,0:T(4,128)(2,1)S(1)}, u32[]{:S(2)}, u32[]{:S(2)}) async-start(bf16[16,3,64]{2,1,0:T(4,128)(2,1)} %all_to_all.72), calls=%async_computation.1 | async-start | bytes 32768 | tf_op jit(solution)/shard_map/all_to_all | solution.py:77
  39.4 1.5 convolution_convert_fusion.5
  40.9 1.2 convolution_convert_fusion.6
  42.7 1.5 convolution_convert_fusion.4
  46.3 6.0 %all-to-all-start.2 = ((bf16[16,3,64]{2,1,0:T(4,128)(2,1)}), bf16[16,3,64]{2,1,0:T(4,128)(2,1)S(1)}, u32[]{:S(2)}, u32[]{:S(2)}) async-start(bf16[16,3,64]{2,1,0:T(4,128)(2,1)} %all_to_all.76), calls=%async_computation.2 | async-start | bytes 32768 | tf_op jit(solution)/shard_map/all_to_all | solution.py:78
  53.0 5.8 %all-to-all-done.2 = bf16[16,3,64]{2,1,0:T(4,128)(2,1)S(1)} async-done(((bf16[16,3,64]{2,1,0:T(4,128)(2,1)}), bf16[16,3,64]{2,1,0:T(4,128)(2,1)S(1)}, u32[]{:S(2)}, u32[]{:S(2)}) %all-to-all-start.2) | async-done | bytes 6176 | tf_op jit(solution)/shard_map/all_to_all | solution.py:78
  58.7 3.5 %all-to-all-start = ((bf16[16,3,256]{2,1,0:T(4,128)(2,1)}), bf16[16,3,256]{2,1,0:T(4,128)(2,1)S(1)}, u32[]{:S(2)}, u32[]{:S(2)}) async-start(bf16[16,3,256]{2,1,0:T(4,128)(2,1)} %all_to_all.68), calls=%async_computation | async-start | bytes 65536 | tf_op jit(solution)/shard_map/all_to_all | solution.py:76
  64.7 4.2 %all-to-all-done = bf16[16,3,256]{2,1,0:T(4,128)(2,1)S(1)} async-done(((bf16[16,3,256]{2,1,0:T(4,128)(2,1)}), bf16[16,3,256]{2,1,0:T(4,128)(2,1)S(1)}, u32[]{:S(2)}, u32[]{:S(2)}) %all-to-all-start) | async-done | bytes 24608 | tf_op jit(solution)/shard_map/all_to_all | solution.py:76
  68.9 3.5 %all-to-all-start.3 = ((bf16[16,3,256]{2,1,0:T(4,128)(2,1)}), bf16[16,3,256]{2,1,0:T(4,128)(2,1)S(1)}, u32[]{:S(2)}, u32[]{:S(2)}) async-start(bf16[16,3,256]{2,1,0:T(4,128)(2,1)} %all_to_all.80), calls=%async_computation.3 | async-start | bytes 65536 | tf_op jit(solution)/shard_map/all_to_all | solution.py:75
  74.7 4.2 %all-to-all-done.3 = bf16[16,3,256]{2,1,0:T(4,128)(2,1)S(1)} async-done(((bf16[16,3,256]{2,1,0:T(4,128)(2,1)}), bf16[16,3,256]{2,1,0:T(4,128)(2,1)S(1)}, u32[]{:S(2)}, u32[]{:S(2)}) %all-to-all-start.3) | async-done | bytes 24608 | tf_op jit(solution)/shard_map/all_to_all | solution.py:75
  79.2 16.8 %fusion = f32[3,8,1,8,64]{4,2,3,1,0:T(1,128)S(1)} fusion(f32[3,8,128,1,1]{2,3,4,1,0:T(1,128)S(1)} %bitcast.105, f32[3,8,8,64,128]{4,3,2,1,0:T(8,128)} %bitcast.96, f32[3,8,128]{2,1,0:T(8,128)S(1)} %bitcast.102, f32[3,8,8,64]{3,2,1,0:T(8,128)S(1)} %broadcast_multiply_fusion.1, f32[3,8,8]{2,1,0:T(8,128)S(1)} %mul.238), kind=kOutput, calls=%fused_computation.4 | convolution fusion | flops 23592960 | bytes 6415104 | tf_op jit(solution)/shard_map/sgepn,sgn->sgep/dot_general | solution.py:107
  96.5 19.0 %all-gather.1 = bf16[16,3,4096]{2,1,0:T(4,128)(2,1)S(1)} all-gather(bf16[1,3,4096]{2,1,0:T(4,128)(2,1)S(1)} %fusion.40), channel_id=1, replica_groups=mesh['grp'=2,'ep'=16] {'ep'}, dimensions={0}, use_global_device_ids=true | all-gather | bytes 417792 | tf_op jit(solution)/shard_map/all_gather | solution.py:118
  115.9 1.5 fusion.21
  120.8 3.5 %all-to-all-start.4 = ((bf16[16,3,128]{2,1,0:T(4,128)(2,1)}), bf16[16,3,128]{2,1,0:T(4,128)(2,1)S(1)}, u32[]{:S(2)}, u32[]{:S(2)}) async-start(bf16[16,3,128]{2,1,0:T(4,128)(2,1)} %all_to_all.82), calls=%async_computation.4 | async-start | bytes 32768 | tf_op jit(solution)/shard_map/all_to_all | solution.py:131
  125.3 7.0 %multiply_add_fusion = f32[3,64,64,128]{3,2,1,0:T(8,128)} fusion(f32[3,64,64,128]{3,2,1,0:T(8,128)} %param.28, f32[3,64,128]{2,1,0:T(8,128)S(1)} %broadcast_bitcast_fusion, f32[3,64,64]{2,1,0:T(8,128)S(1)} %broadcast_multiply_fusion, f32[3,64]{1,0:T(4,128)S(1)} %get-tuple-element.11), kind=kLoop, calls=%fused_computation.3 | loop fusion | flops 4718592 | bytes 12731136 | tf_op jit(solution)/shard_map/add | solution.py:104
  133.4 6.0 %all-to-all-start.5 = ((bf16[16,1,2,2048]{3,2,1,0:T(2,128)(2,1)}), bf16[16,1,2,2048]{3,2,1,0:T(2,128)(2,1)S(1)}, u32[]{:S(2)}, u32[]{:S(2)}) async-start(bf16[16,1,2,2048]{3,2,1,0:T(2,128)(2,1)} %bitcast.18), calls=%async_computation.5 | async-start | bytes 262144 | tf_op jit(solution)/shard_map/all_to_all | solution.py:151
  140.7 6.7 %all-to-all-done.5 = bf16[16,1,2,2048]{3,2,1,0:T(2,128)(2,1)S(1)} async-done(((bf16[16,1,2,2048]{3,2,1,0:T(2,128)(2,1)}), bf16[16,1,2,2048]{3,2,1,0:T(2,128)(2,1)S(1)}, u32[]{:S(2)}, u32[]{:S(2)}) %all-to-all-start.5) | async-done | bytes 131104 | tf_op jit(solution)/shard_map/all_to_all | solution.py:151
  147.4 2.0 fusion.11
  149.4 2.5 %convolution_convert_fusion = bf16[32,2048]{1,0:T(8,128)(2,1)S(1)} fusion(bf16[1,512,2048]{2,1,0:T(8,128)(2,1)S(1)} %copy-done, bf16[32,2048]{1,0:T(8,128)(2,1)S(1)} %reshape_squeeze.3, bf16[1,2048,512]{2,1,0:T(8,128)(2,1)} %param.47, f32[32,512]{1,0:T(8,128)S(1)} %fusion.11), kind=kOutput, calls=%fused_computation.11 | convolution fusion | flops 134381568 | bytes 4521984 | tf_op jit(solution)/shard_map/dot_general | solution.py:21
  152.7 3.5 %all-to-all-start.6 = ((bf16[16,1,2,2048]{3,2,1,0:T(2,128)(2,1)}), bf16[16,1,2,2048]{3,2,1,0:T(2,128)(2,1)S(1)}, u32[]{:S(2)}, u32[]{:S(2)}) async-start(bf16[16,1,2,2048]{3,2,1,0:T(2,128)(2,1)} %bitcast.22), calls=%async_computation.6 | async-start | bytes 262144 | tf_op jit(solution)/shard_map/all_to_all | solution.py:155
  156.3 52.1 %all-reduce.3.cloned.1.call-done = bf16[48,1024]{1,0:T(8,128)(2,1)} async-done(((bf16[48,1024]{1,0:T(8,128)(2,1)}), bf16[48,1024]{1,0:T(8,128)(2,1)}) %all-reduce.3.cloned.1.call-update) | async-done | bytes 98320
  210.1 2.6 %fusion.7 = bf16[3,2048]{1,0:T(4,128)(2,1)} fusion(bf16[512,2048]{1,0:T(8,128)(2,1)} %param.51, f32[3,2048]{1,0:T(4,128)S(1)} %multiply_reduce_fusion.2, bf16[16,3,128]{2,1,0:T(4,128)(2,1)S(1)} %all-to-all-done.4, f32[3,1024]{1,0:T(4,128)S(1)} %dynamic-slice_convert_fusion, f32[3]{0:T(128)S(1)} %add_rsqrt_fusion.1), kind=kOutput, calls=%fused_computation.14 | convolution fusion | flops 6328320 | bytes 2158604 | tf_op jit(solution)/shard_map/dot_general | solution.py:21
  (108 shorter events, 20.9 us)
Async XLA Ops:
  7.2 142.3 %copy-start = (bf16[1,512,2048]{2,1,0:T(8,128)(2,1)S(1)}, bf16[1,512,2048]{2,1,0:T(8,128)(2,1)}, u32[]{:S(2)}) copy-start(bf16[1,512,2048]{2,1,0:T(8,128)(2,1)} %param.48) | copy-start | bytes 6291460
  7.2 56.1 %copy-start.12 = (u32[32]{0:T(128)S(1)}, u32[32]{0:T(128)}, u32[]{:S(2)}) copy-start(u32[32]{0:T(128)} %constant.128) | copy-start | bytes 388
  7.2 38.1 %copy-start.3 = (s32[3,6]{1,0:T(4,128)S(1)}, s32[3,6]{1,0:T(4,128)}, u32[]{:S(2)}) copy-start(s32[3,6]{1,0:T(4,128)} %param.45) | copy-start | bytes 220
  7.2 38.2 %copy-start.2 = (bf16[2048,64]{0,1:T(8,128)(2,1)S(1)}, bf16[2048,64]{0,1:T(8,128)(2,1)}, u32[]{:S(2)}) copy-start(bf16[2048,64]{0,1:T(8,128)(2,1)} %param.33) | copy-start | bytes 786436
  7.2 38.2 %copy-start.9 = (f32[64]{0:T(128)S(1)}, f32[64]{0:T(128)}, u32[]{:S(2)}) copy-start(f32[64]{0:T(128)} %param.34) | copy-start | bytes 772
  7.2 38.2 %copy-start.8 = (f32[3,64]{1,0:T(4,128)S(1)}, f32[3,64]{1,0:T(4,128)}, u32[]{:S(2)}) copy-start(f32[3,64]{1,0:T(4,128)} %param.36) | copy-start | bytes 2308
  7.2 55.0 %copy-start.4 = (bf16[4,6144]{1,0:T(4,128)(2,1)S(1)}, bf16[4,6144]{1,0:T(4,128)(2,1)}, u32[]{:S(2)}) copy-start(bf16[4,6144]{1,0:T(4,128)(2,1)} %param.38) | copy-start | bytes 147460
  7.2 55.8 %copy-start.10 = (f32[64]{0:T(128)S(1)}, f32[64]{0:T(128)}, u32[]{:S(2)}) copy-start(f32[64]{0:T(128)} %param.37) | copy-start | bytes 772
  7.3 55.9 %copy-start.7 = (f32[2048]{0:T(1024)S(1)}, f32[2048]{0:T(1024)}, u32[]{:S(2)}) copy-start(f32[2048]{0:T(1024)} %param.43) | copy-start | bytes 24580
  7.3 65.2 %copy-start.1 = (bf16[3,3,6144]{2,1,0:T(4,128)(2,1)S(1)}, bf16[3,3,6144]{2,1,0:T(4,128)(2,1)}, u32[]{:S(2)}) copy-start(bf16[3,3,6144]{2,1,0:T(4,128)(2,1)} %param.27) | copy-start | bytes 331780
  7.3 66.4 %copy-start.5 = (f32[6144]{0:T(1024)S(1)}, f32[6144]{0:T(1024)}, u32[]{:S(2)}) copy-start(f32[6144]{0:T(1024)} %param.39) | copy-start | bytes 73732
  34.4 11.9 %all-to-all-start.1 = ((bf16[16,3,64]{2,1,0:T(4,128)(2,1)}), bf16[16,3,64]{2,1,0:T(4,128)(2,1)S(1)}, u32[]{:S(2)}, u32[]{:S(2)}) async-start(bf16[16,3,64]{2,1,0:T(4,128)(2,1)} %all_to_all.72), calls=%async_computation.1 | async-start | bytes 32768 | tf_op jit(solution)/shard_map/all_to_all | solution.py:77
  44.4 52.0 %copy-start.6 = (f32[4096]{0:T(1024)S(1)}, f32[4096]{0:T(1024)}, u32[]{:S(2)}) copy-start(f32[4096]{0:T(1024)} %param.41) | copy-start | bytes 49156
  46.3 12.5 %all-to-all-start.2 = ((bf16[16,3,64]{2,1,0:T(4,128)(2,1)}), bf16[16,3,64]{2,1,0:T(4,128)(2,1)S(1)}, u32[]{:S(2)}, u32[]{:S(2)}) async-start(bf16[16,3,64]{2,1,0:T(4,128)(2,1)} %all_to_all.76), calls=%async_computation.2 | async-start | bytes 32768 | tf_op jit(solution)/shard_map/all_to_all | solution.py:78
  58.7 10.1 %all-to-all-start = ((bf16[16,3,256]{2,1,0:T(4,128)(2,1)}), bf16[16,3,256]{2,1,0:T(4,128)(2,1)S(1)}, u32[]{:S(2)}, u32[]{:S(2)}) async-start(bf16[16,3,256]{2,1,0:T(4,128)(2,1)} %all_to_all.68), calls=%async_computation | async-start | bytes 65536 | tf_op jit(solution)/shard_map/all_to_all | solution.py:76
  68.9 10.1 %all-to-all-start.3 = ((bf16[16,3,256]{2,1,0:T(4,128)(2,1)}), bf16[16,3,256]{2,1,0:T(4,128)(2,1)S(1)}, u32[]{:S(2)}, u32[]{:S(2)}) async-start(bf16[16,3,256]{2,1,0:T(4,128)(2,1)} %all_to_all.80), calls=%async_computation.3 | async-start | bytes 65536 | tf_op jit(solution)/shard_map/all_to_all | solution.py:75
  72.4 136.1 %all-reduce.3.cloned.1.call-start = ((), (), s32[]{:S(2)}) async-start(), calls=%async_computation.7 | async-start | bytes 196608
  120.8 11.5 %all-to-all-start.4 = ((bf16[16,3,128]{2,1,0:T(4,128)(2,1)}), bf16[16,3,128]{2,1,0:T(4,128)(2,1)S(1)}, u32[]{:S(2)}, u32[]{:S(2)}) async-start(bf16[16,3,128]{2,1,0:T(4,128)(2,1)} %all_to_all.82), calls=%async_computation.4 | async-start | bytes 32768 | tf_op jit(solution)/shard_map/all_to_all | solution.py:131
  125.3 14.1 %copy-start.11 = (bf16[2048,16]{0,1:T(8,128)(2,1)S(1)}, bf16[2048,16]{0,1:T(8,128)(2,1)}, u32[]{:S(2)}) copy-start(bf16[2048,16]{0,1:T(8,128)(2,1)} %param.44) | copy-start | bytes 196612
  133.4 13.9 %all-to-all-start.5 = ((bf16[16,1,2,2048]{3,2,1,0:T(2,128)(2,1)}), bf16[16,1,2,2048]{3,2,1,0:T(2,128)(2,1)S(1)}, u32[]{:S(2)}, u32[]{:S(2)}) async-start(bf16[16,1,2,2048]{3,2,1,0:T(2,128)(2,1)} %bitcast.18), calls=%async_computation.5 | async-start | bytes 262144 | tf_op jit(solution)/shard_map/all_to_all | solution.py:151
  152.7 56.5 %all-to-all-start.6 = ((bf16[16,1,2,2048]{3,2,1,0:T(2,128)(2,1)}), bf16[16,1,2,2048]{3,2,1,0:T(2,128)(2,1)S(1)}, u32[]{:S(2)}, u32[]{:S(2)}) async-start(bf16[16,1,2,2048]{3,2,1,0:T(2,128)(2,1)} %bitcast.22), calls=%async_computation.6 | async-start | bytes 262144 | tf_op jit(solution)/shard_map/all_to_all | solution.py:155
Sparse Core Ops, SparseCore 0:
  120.9 87.4 all-reduce.2
where the time goes:
time: 221 us; the launch traced here: 220 us
  waiting for transfers between devices  73 us (33%)
  blocking collectives  43.3 us (20%)
  matrix products  33.5 us (15%)
  starting transfers between devices  29.5 us (13%)
  between operations  15.2 us (7%)
  other arithmetic  14.1 us (6%)
  local copies, waits for them, and re-layouts  11 us (5%)
    unnamed x2, waiting for transfers between devices  52.2 us
    all_gather x1, blocking collectives, shards(): gathered = lax.all_gather(hidden, 'ep', axis=0, tiled=True)  24.2 us
    all_gather x1, blocking collectives, shards(): lax.all_gather(gated_out, 'ep', axis=0, tiled=True)  19 us
    dot_general x13, matrix products, matmul(): return jnp.dot(left, right, preferred_element_type=jnp.float32)  16.8 us
    dot_general x1, matrix products, shards(): jnp.einsum('sgepn,sgn->sgep', next_state, read_vec, precision=lax.Precisi...  16.8 us
    add x1, other arithmetic, shards(): decay_rate[..., None, None] * carried  6.99 us
    all_to_all x1, waiting for transfers between devices, shards(): lax.all_to_all(outbound, 'ep', split_axis=0, concat_axis=0, tiled=True)  6.66 us
    all_to_all x1, starting transfers between devices, shards(): lax.all_to_all(read_part, 'ep', split_axis=0, concat_axis=1, tiled=True)  5.97 us
  transfers between devices with their start and end apart: 8, of which 5 were waited for; matrix products, arithmetic and copies ran while one was open for 13% of the time, Pallas kernels for 0%

commit v1 on v0

v1 whole, which is shorter than its diff:
```python
import functools

import jax
import jax.numpy as jnp
from jax import lax
from jax.experimental import pallas as pl
from jax.experimental.pallas import tpu as pltpu
from jax.sharding import PartitionSpec as P

HEAD_DIM = 64
GROUPS = 8
STATE = 128


epsilon = 1e-06
routed_scale = 2.5


def row_scale(values):
    return lax.rsqrt(jnp.mean(values * values, axis=-1, keepdims=True) + epsilon)


def matmul(left, right):
    return jnp.dot(left, right, preferred_element_type=jnp.float32)


def expert_result(rows_in, weight_gate, weight_up, weight_down):
    expert_hidden = (jax.nn.silu(matmul(rows_in, weight_gate)) * matmul(rows_in, weight_up)).astype(
        jnp.bfloat16
    )
    return matmul(expert_hidden, weight_down).astype(jnp.bfloat16)


def exchange(blocks, ident):
    return lax.all_to_all(blocks, "ep", split_axis=0, concat_axis=0, tiled=True)


def gather(block, ident):
    return exchange(jnp.broadcast_to(block[None], (lax.axis_size("ep"),) + block.shape), ident)


def state_kernel(per_group, decay, inputs, write, read, carried, updated, mixed):
    row, part = pl.program_id(0), pl.program_id(1)
    heads = carried.shape[1]
    scaled = inputs[0, 0]
    lane = lax.broadcasted_iota(jnp.int32, scaled.shape, 1)
    total = jnp.zeros(scaled.shape, jnp.float32)
    for head in range(heads):
        group = head // per_group
        fresh = (
            carried[0, head] * decay[row, part * heads + head]
            + scaled[:, head : head + 1] * write[0, 0, group : group + 1]
        )
        updated[0, head] = fresh
        column = jnp.sum(fresh * read[0, 0, group : group + 1], axis=1, keepdims=True)
        total = jnp.where(lane == head, column, total)
    mixed[0, 0] = total


def state_step(state, decay_rate, scaled, write_vec, read_vec):
    rows, head_count, head_dim, entries = state.shape
    groups = write_vec.shape[1]
    parts = 2
    heads = head_count // parts
    inputs = scaled.reshape(rows, parts, heads, head_dim).transpose(0, 1, 3, 2)
    vec_shape = (rows, parts, groups // parts, entries)
    part_spec = lambda *dims: pl.BlockSpec((1, 1) + dims, lambda row, part: (row, part, 0, 0))
    state_spec = pl.BlockSpec((1, heads, head_dim, entries), lambda row, part: (row, part, 0, 0))
    next_state, mixed = pl.pallas_call(
        functools.partial(state_kernel, head_count // groups),
        grid=(rows, parts),
        out_shape=(
            jax.ShapeDtypeStruct(state.shape, jnp.float32),
            jax.ShapeDtypeStruct(inputs.shape, jnp.float32),
        ),
        in_specs=[
            pl.BlockSpec(memory_space=pltpu.SMEM),
            part_spec(head_dim, heads),
            part_spec(groups // parts, entries),
            part_spec(groups // parts, entries),
            state_spec,
        ],
        out_specs=(state_spec, part_spec(head_dim, heads)),
    )(decay_rate, inputs, write_vec.reshape(vec_shape), read_vec.reshape(vec_shape), state)
    return next_state, mixed.transpose(0, 1, 3, 2).reshape(rows, head_count, head_dim)


def shards(
    hidden,
    conv_window,
    ssm_state,
    gate_proj,
    input_proj,
    write_proj,
    read_proj,
    step_proj,
    step_bias,
    decay_log,
    decay_shift,
    skip_scale,
    conv_taps,
    conv_bias,
    mix_gain,
    group_gain,
    out_proj,
    ffn_gain,
    router,
    expert_ids,
    expert_gate,
    expert_up,
    expert_down,
    shared_gate,
    shared_up,
    shared_down,
):
    local_rows = hidden.shape[0]
    device_index = lax.axis_index("ep")
    width = hidden.shape[1]
    first_row = device_index * local_rows
    gathered = gather(hidden, 0).reshape(-1, width)
    gathered_wide = gathered.astype(jnp.float32)
    normed = (gathered_wide * row_scale(gathered_wide) * mix_gain).astype(jnp.bfloat16)
    parts = [matmul(normed, proj).astype(jnp.bfloat16) for proj in (gate_proj, input_proj, write_proj, read_proj)]
    outbound = jnp.concatenate(parts, axis=1)
    arrived = exchange(outbound.reshape(-1, local_rows, outbound.shape[1]), 1)
    rows, offset = [], 0
    for part in parts:
        piece = arrived[:, :, offset : offset + part.shape[1]]
        rows.append(piece.transpose(1, 0, 2).reshape(local_rows, -1))
        offset += part.shape[1]
    gate_rows, input_rows, write_rows, read_rows = rows
    hidden_wide = hidden.astype(jnp.float32)
    normed_local = (hidden_wide * row_scale(hidden_wide) * mix_gain).astype(jnp.bfloat16)
    step_raw = matmul(normed_local, step_proj)
    inner_width = gate_rows.shape[1]
    state_span = GROUPS * STATE
    head_count = step_bias.shape[0]
    fresh_row = jnp.concatenate([input_rows, write_rows, read_rows], axis=1)
    window = jnp.concatenate([conv_window, fresh_row[:, None, :]], axis=1)
    convolved = jax.nn.silu(
        jnp.sum(window.astype(jnp.float32) * conv_taps.astype(jnp.float32)[None], axis=1)
        + conv_bias
    )
    head_input = convolved[:, :inner_width].reshape(local_rows, head_count, HEAD_DIM)
    write_vec = convolved[:, inner_width : inner_width + state_span].reshape(
        local_rows, GROUPS, STATE
    )
    read_vec = convolved[:, inner_width + state_span :].reshape(local_rows, GROUPS, STATE)
    step_size = jax.nn.softplus(step_raw + step_bias)
    decay_rate = jnp.exp(decay_shift - step_size * jnp.exp(decay_log))
    next_state, mixed_out = state_step(
        ssm_state, decay_rate, step_size[:, :, None] * head_input, write_vec, read_vec
    )
    mixed_out = mixed_out + skip_scale[None, :, None] * head_input
    mixed_out = mixed_out.reshape(local_rows, inner_width).astype(jnp.bfloat16)
    gated_out = mixed_out.astype(jnp.float32) * jax.nn.silu(gate_rows.astype(jnp.float32))
    blocks = gated_out.reshape(local_rows, GROUPS, -1)
    gated_out = ((blocks * row_scale(blocks)).reshape(local_rows, inner_width) * group_gain).astype(
        jnp.bfloat16
    )
    col_width = out_proj.shape[1]
    resid_cols = lax.dynamic_slice_in_dim(gathered_wide, device_index * col_width, col_width, 1)
    resid_part = (
        resid_cols + matmul(gather(gated_out, 2).reshape(-1, inner_width), out_proj)
    ).astype(jnp.bfloat16)
    resid_all = gather(resid_part, 3).transpose(1, 0, 2).reshape(-1, width)
    gain_part = lax.dynamic_slice_in_dim(ffn_gain, device_index * col_width, col_width, 0)
    shared_part = (resid_part.astype(jnp.float32) * gain_part).astype(jnp.bfloat16)
    shared_pre = jnp.concatenate(
        [matmul(shared_part, shared_gate), matmul(shared_part, shared_up)], axis=1
    ).astype(jnp.bfloat16)
    resid_all_wide = resid_all.astype(jnp.float32)
    scale_all = row_scale(resid_all_wide)
    routed_all = (resid_all_wide * scale_all * ffn_gain).astype(jnp.bfloat16)
    result = expert_result(routed_all, expert_gate[0], expert_up[0], expert_down[0])
    back = exchange(
        jnp.concatenate([result, shared_pre], axis=1).reshape(
            -1, local_rows, width + shared_pre.shape[1]
        ),
        4,
    ).astype(jnp.float32)
    resid_wide = lax.dynamic_slice_in_dim(resid_all_wide, first_row, local_rows, 0)
    norm_scale = lax.dynamic_slice_in_dim(scale_all, first_row, local_rows, 0)
    routed_in = lax.dynamic_slice_in_dim(routed_all, first_row, local_rows, 0)
    scores = jax.nn.sigmoid(matmul(routed_in, router))
    chosen = jnp.any(
        expert_ids[:, :, None] == jnp.arange(router.shape[1], dtype=jnp.int32)[None, None, :], axis=1
    )
    scores = jnp.where(chosen, scores, 0.0)
    weights = routed_scale * scores / jnp.sum(scores, axis=1, keepdims=True)
    routed = jnp.sum(back[:, :, :width] * weights.T[:, :, None], axis=0)
    shared_sum = jnp.sum(back[:, :, width:], axis=0)
    hidden_units = shared_down.shape[0]
    shared_hidden = (
        jax.nn.silu(norm_scale * shared_sum[:, :hidden_units])
        * (norm_scale * shared_sum[:, hidden_units:])
    ).astype(jnp.bfloat16)
    layer_out = (resid_wide + routed + matmul(shared_hidden, shared_down)).astype(jnp.bfloat16)
    return (layer_out, next_state, window[:, 1:])


def solution(mesh):
    placed = (
        P(("grp", "ep"), None),
        P(("grp", "ep"), None, None),
        P(("grp", "ep"), None, None, None),
        P(None, "ep"),
        P(None, "ep"),
        P(None, "ep"),
        P(None, "ep"),
        P(),
        P(),
        P(),
        P(("grp", "ep"), None),
        P(),
        P(),
        P(),
        P(),
        P(),
        P(None, "ep"),
        P(),
        P(),
        P(("grp", "ep"), None),
        P("ep", None, None),
        P("ep", None, None),
        P("ep", None, None),
        P("ep", None),
        P("ep", None),
        P(),
    )
    return jax.shard_map(
        shards,
        mesh=mesh,
        in_specs=placed,
        out_specs=(
            P(("grp", "ep"), None),
            P(("grp", "ep"), None, None, None),
            P(("grp", "ep"), None, None),
        ),
        check_vma=False,
    )
```

time: 221 us -> 119 us (0.54)
  blocking collectives: 43.3 us -> 0 us
  waiting for transfers between devices: 73 us -> 47.8 us
  matrix products: 33.5 us -> 12.6 us
  Pallas kernels: 0 us -> 19.4 us
  between operations: 15.2 us -> 1.14 us
  other arithmetic: 14.1 us -> 4.91 us
  starting transfers between devices: 29.5 us -> 22.3 us
    unnamed x2 -> x0, waiting for transfers between devices: 52.2 us -> none
    all_gather x2 -> x0, blocking collectives: 43.3 us -> none  [the longest x1 24.2 us: shards(): gathered = lax.all_gather(hidden, 'ep', axis=0, tiled=True)]
    all_to_all x7 -> x5, waiting for transfers between devices: 20.8 us -> 47.8 us  [exchange(): return lax.all_to_all(blocks, 'ep', split_axis=0, concat_axis=0, tiled=True)]
    pallas_call x0 -> x1, Pallas kernels: none -> 19.4 us  [state_step(): pl.pallas_call(functools.partial(state_kernel, head_count // groups), gri...]
    dot_general x1 -> x0, matrix products: 16.8 us -> none  [shards(): jnp.einsum('sgepn,sgn->sgep', next_state, read_vec, precision=lax.Precisi...]
    all_to_all x7 -> x5, starting transfers between devices: 29.4 us -> 22.3 us  [exchange(): return lax.all_to_all(blocks, 'ep', split_axis=0, concat_axis=0, tiled=True)]
    add x1 -> x0, other arithmetic: 6.99 us -> none  [shards(): decay_rate[..., None, None] * carried]
    dot_general x13 -> x12, matrix products: 16.8 us -> 12.6 us  [matmul(): return jnp.dot(left, right, preferred_element_type=jnp.float32)]
  transfers between devices with their start and end apart: 8 -> 5, of which waited for: 5 -> 5; matrix products, arithmetic and copies ran while one was open for 13% -> 4% of each run, Pallas kernels for 0% -> 0%
where the time goes in v1:
time: 119 us; the launch traced here: 118 us
  waiting for transfers between devices  47.8 us (40%)
  starting transfers between devices  22.3 us (19%)
  Pallas kernels  19.4 us (16%)
  matrix products  12.6 us (11%)
  local copies, waits for them, and re-layouts  9.86 us (8%)
  other arithmetic  4.91 us (4%)
    all_to_all x5, waiting for transfers between devices, exchange(): return lax.all_to_all(blocks, 'ep', split_axis=0, concat_axis=0, tiled=True)  47.8 us
    all_to_all x5, starting transfers between devices, exchange(): return lax.all_to_all(blocks, 'ep', split_axis=0, concat_axis=0, tiled=True)  22.3 us
    pallas_call x1, Pallas kernels, state_step(): pl.pallas_call(functools.partial(state_kernel, head_count // groups), gri...  19.4 us
    dot_general x12, matrix products, matmul(): return jnp.dot(left, right, preferred_element_type=jnp.float32)  12.6 us
    broadcast_in_dim x3, local copies, waits for them, and re-layouts, gather(): jnp.broadcast_to(block[None], (lax.axis_size('ep'),) + block.shape)  3.39 us
  transfers between devices with their start and end apart: 5, of which 5 were waited for; matrix products, arithmetic and copies ran while one was open for 4% of the time, Pallas kernels for 0%

profile of v1, /device:TPU:0, one launch (start us, length us, event | category | flops | bytes accessed | tf_op | source)
XLA Modules:
  0.0 118.0 jit_solution(9285674787470805963)
XLA Ops:
  0.7 1.7 %broadcast_in_dim.13 = bf16[16,3,2048]{2,1,0:T(4,128)(2,1)} broadcast(bf16[3,2048]{1,0:T(4,128)(2,1)} %param.26), dimensions={1,2} | broadcast | bytes 208896 | tf_op jit(solution)/shard_map/broadcast_in_dim | solution.py:39
  2.3 7.4 %all-to-all-start = ((bf16[16,3,2048]{2,1,0:T(4,128)(2,1)}), bf16[16,3,2048]{2,1,0:T(4,128)(2,1)S(1)}, u32[]{:S(2)}, u32[]{:S(2)}) async-start(bf16[16,3,2048]{2,1,0:T(4,128)(2,1)} %broadcast_in_dim.13), calls=%async_computation | async-start | bytes 524288 | tf_op jit(solution)/shard_map/all_to_all | solution.py:35
  10.4 0.9 fusion.38
  11.3 8.5 %all-to-all-done = bf16[16,3,2048]{2,1,0:T(4,128)(2,1)S(1)} async-done(((bf16[16,3,2048]{2,1,0:T(4,128)(2,1)}), bf16[16,3,2048]{2,1,0:T(4,128)(2,1)S(1)}, u32[]{:S(2)}, u32[]{:S(2)}) %all-to-all-start) | async-done | bytes 196640 | tf_op jit(solution)/shard_map/all_to_all | solution.py:35
  20.3 0.9 multiply_convert_fusion
  21.8 1.6 %convolution_convert_fusion.3 = bf16[48,256]{1,0:T(8,128)(2,1)S(1)} fusion(bf16[48,2048]{1,0:T(8,128)(2,1)S(1)} %multiply_convert_fusion, bf16[2048,256]{1,0:T(8,128)(2,1)} %param.30), kind=kOutput, calls=%fused_computation.12 | convolution fusion | flops 50343936 | bytes 1269760 | tf_op jit(solution)/shard_map/dot_general | solution.py:24
  24.4 3.5 %all-to-all-start.1 = ((bf16[16,3,640]{2,1,0:T(4,128)(2,1)}), bf16[16,3,640]{2,1,0:T(4,128)(2,1)S(1)}, u32[]{:S(2)}, u32[]{:S(2)}) async-start(bf16[16,3,640]{2,1,0:T(4,128)(2,1)} %reshape.143), calls=%async_computation.1 | async-start | bytes 163840 | tf_op jit(solution)/shard_map/all_to_all | solution.py:35
  27.9 0.8 subtract_exponential_fusion
  29.1 5.9 %all-to-all-done.1 = bf16[16,3,640]{2,1,0:T(4,128)(2,1)S(1)} async-done(((bf16[16,3,640]{2,1,0:T(4,128)(2,1)}), bf16[16,3,640]{2,1,0:T(4,128)(2,1)S(1)}, u32[]{:S(2)}, u32[]{:S(2)}) %all-to-all-start.1) | async-done | bytes 61472 | tf_op jit(solution)/shard_map/all_to_all | solution.py:35
  38.0 19.4 %shard_map.265 = (f32[3,64,64,128]{3,2,1,0:T(8,128)}, f32[3,2,64,32]{3,2,1,0:T(8,128)}) custom-call(f32[3,64]{1,0:T(4,128)} %get-tuple-element.15.decay, f32[3,2,64,32]{3,2,1,0:T(8,128)} %multiply_bitcast_fusion.inputs, f32[3,2,4,128]{3,2,1,0:T(4,128)} %reshape_reshape.6.write, f32[3,2,4,128]{3,2,1,0:T(4,128)} %reshape_reshape.7.read, f32[3,64,64,128]{3,2,1,0:T(8,128)} %carried.1), custom_call_target="tpu_custom_call" | custom-call | tf_op jit(solution)/shard_map/pallas_call | solution.py:69
  57.4 1.0 copy.61
  58.9 1.0 broadcast_in_dim.15
  59.9 3.7 %all-to-all-start.2 = ((bf16[16,3,4096]{2,1,0:T(4,128)(2,1)}), bf16[16,3,4096]{2,1,0:T(4,128)(2,1)S(1)}, u32[]{:S(2)}, u32[]{:S(2)}) async-start(bf16[16,3,4096]{2,1,0:T(4,128)(2,1)} %broadcast_in_dim.15), calls=%async_computation.2 | async-start | bytes 1048576 | tf_op jit(solution)/shard_map/all_to_all | solution.py:35
  63.7 0.9 fusion.30
  64.6 13.3 %all-to-all-done.2 = bf16[16,3,4096]{2,1,0:T(4,128)(2,1)S(1)} async-done(((bf16[16,3,4096]{2,1,0:T(4,128)(2,1)}), bf16[16,3,4096]{2,1,0:T(4,128)(2,1)S(1)}, u32[]{:S(2)}, u32[]{:S(2)}) %all-to-all-start.2) | async-done | bytes 393248 | tf_op jit(solution)/shard_map/all_to_all | solution.py:35
  78.2 1.6 %fusion.14 = bf16[48,128]{1,0:T(8,128)(2,1)S(1)} fusion(bf16[48,4096]{1,0:T(8,128)(2,1)S(1)} %reshape.149, bf16[4096,128]{1,0:T(8,128)(2,1)} %param.42, f32[48,2048]{1,0:T(8,128)S(1)} %reshape.151, s32[]{:T(128)S(6)} %select_n.20), kind=kOutput, calls=%fused_computation.15 | convolution fusion | flops 50343936 | bytes 1478660 | tf_op jit(solution)/shard_map/dot_general | solution.py:24
  80.5 4.1 %all-to-all-start.3 = ((bf16[16,48,128]{2,1,0:T(8,128)(2,1)}), bf16[16,48,128]{2,1,0:T(8,128)(2,1)S(1)}, u32[]{:S(2)}, u32[]{:S(2)}) async-start(bf16[16,48,128]{2,1,0:T(8,128)(2,1)} %broadcast_in_dim.16), calls=%async_computation.3 | async-start | bytes 393216 | tf_op jit(solution)/shard_map/all_to_all | solution.py:35
  84.9 8.7 %all-to-all-done.3 = bf16[16,48,128]{2,1,0:T(8,128)(2,1)S(1)} async-done(((bf16[16,48,128]{2,1,0:T(8,128)(2,1)}), bf16[16,48,128]{2,1,0:T(8,128)(2,1)S(1)}, u32[]{:S(2)}, u32[]{:S(2)}) %all-to-all-start.3) | async-done | bytes 196640 | tf_op jit(solution)/shard_map/all_to_all | solution.py:35
  93.7 2.1 %fusion.4 = f32[48,512]{1,0:T(8,128)S(1)} fusion(bf16[1,2048,512]{2,1,0:T(8,128)(2,1)} %param.46, bf16[16,48,128]{2,1,0:T(8,128)(2,1)S(1)} %all-to-all-done.3, f32[16,128]{1,0:T(8,128)S(1)} %bitcast.81, f32[48]{0:T(128)S(1)} %add_rsqrt_fusion.2), kind=kOutput, calls=%fused_computation.6 | convolution fusion | flops 101056512 | bytes 2400448 | tf_op jit(solution)/shard_map/dot_general | solution.py:24
  95.8 2.5 %convolution_convert_fusion = bf16[48,2048]{1,0:T(8,128)(2,1)S(1)} fusion(bf16[1,512,2048]{2,1,0:T(8,128)(2,1)S(1)} %copy-done, bf16[1,2048,512]{2,1,0:T(8,128)(2,1)} %param.47, f32[48,512]{1,0:T(8,128)S(1)} %fusion.4, bf16[16,48,128]{2,1,0:T(8,128)(2,1)S(1)} %all-to-all-done.3, f32[16,128]{1,0:T(8,128)S(1)} %bitcast.82, f32[48]{0:T(128)S(1)} %add_rsqrt_fusion.2), kind=kOutput, calls=%fused_computation | convolution fusion | flops 201965568 | bytes 4694208 | tf_op jit(solution)/shard_map/dot_general | solution.py:24
  98.4 0.9 reshape.150
  99.3 3.6 %all-to-all-start.4 = ((bf16[16,3,3072]{2,1,0:T(4,128)(2,1)}), bf16[16,3,3072]{2,1,0:T(4,128)(2,1)S(1)}, u32[]{:S(2)}, u32[]{:S(2)}) async-start(bf16[16,3,3072]{2,1,0:T(4,128)(2,1)} %reshape.150), calls=%async_computation.4 | async-start | bytes 786432 | tf_op jit(solution)/shard_map/all_to_all | solution.py:35
  103.5 11.5 %all-to-all-done.4 = bf16[16,3,3072]{2,1,0:T(4,128)(2,1)S(1)} async-done(((bf16[16,3,3072]{2,1,0:T(4,128)(2,1)}), bf16[16,3,3072]{2,1,0:T(4,128)(2,1)S(1)}, u32[]{:S(2)}, u32[]{:S(2)}) %all-to-all-start.4) | async-done | bytes 294944 | tf_op jit(solution)/shard_map/all_to_all | solution.py:35
  115.3 2.6 %fusion = bf16[3,2048]{1,0:T(4,128)(2,1)} fusion(bf16[512,2048]{1,0:T(8,128)(2,1)} %param.51, f32[3,2048]{1,0:T(4,128)S(1)} %fusion.19, f32[48,2048]{1,0:T(8,128)S(1)} %copy_bitcast_fusion, s32[]{:T(128)S(6)} %select_n.22, f32[3,1024]{1,0:T(4,128)S(1)} %slice_reduce_fusion, f32[3]{0:T(128)S(1)} %dynamic-slice.4), kind=kOutput, calls=%fused_computation.2 | convolution fusion | flops 6322176 | bytes 2170896 | tf_op jit(solution)/shard_map/dot_general | solution.py:24
  (94 shorter events, 8.9 us)
Async XLA Ops:
  0.6 95.2 %copy-start = (bf16[1,512,2048]{2,1,0:T(8,128)(2,1)S(1)}, bf16[1,512,2048]{2,1,0:T(8,128)(2,1)}, u32[]{:S(2)}) copy-start(bf16[1,512,2048]{2,1,0:T(8,128)(2,1)} %param.48) | copy-start | bytes 6291460
  0.6 20.5 %copy-start.3 = (bf16[2048,64]{0,1:T(8,128)(2,1)S(1)}, bf16[2048,64]{0,1:T(8,128)(2,1)}, u32[]{:S(2)}) copy-start(bf16[2048,64]{0,1:T(8,128)(2,1)} %param.32) | copy-start | bytes 786436
  0.7 20.8 %copy-start.4 = (bf16[2048,64]{0,1:T(8,128)(2,1)S(1)}, bf16[2048,64]{0,1:T(8,128)(2,1)}, u32[]{:S(2)}) copy-start(bf16[2048,64]{0,1:T(8,128)(2,1)} %param.31) | copy-start | bytes 786436
  2.3 17.4 %all-to-all-start = ((bf16[16,3,2048]{2,1,0:T(4,128)(2,1)}), bf16[16,3,2048]{2,1,0:T(4,128)(2,1)S(1)}, u32[]{:S(2)}, u32[]{:S(2)}) async-start(bf16[16,3,2048]{2,1,0:T(4,128)(2,1)} %broadcast_in_dim.13), calls=%async_computation | async-start | bytes 524288 | tf_op jit(solution)/shard_map/all_to_all | solution.py:35
  20.3 3.1 %copy-start.1 = (bf16[2048,256]{1,0:T(8,128)(2,1)S(1)}, bf16[2048,256]{1,0:T(8,128)(2,1)}, u32[]{:S(2)}) copy-start(bf16[2048,256]{1,0:T(8,128)(2,1)} %param.29) | copy-start | bytes 3145732
  21.2 6.7 %copy-start.7 = (bf16[3,2048]{1,0:T(4,128)(2,1)S(1)}, bf16[3,2048]{1,0:T(4,128)(2,1)}, u32[]{:S(2)}) copy-start(bf16[3,2048]{1,0:T(4,128)(2,1)} %param.26) | copy-start | bytes 36868
  21.2 6.7 %copy-start.12 = (f32[2048]{0:T(1024)S(1)}, f32[2048]{0:T(1024)}, u32[]{:S(2)}) copy-start(f32[2048]{0:T(1024)} %param.40) | copy-start | bytes 24580
  21.2 6.7 %copy-start.15 = (bf16[2048,64]{0,1:T(8,128)(2,1)S(1)}, bf16[2048,64]{0,1:T(8,128)(2,1)}, u32[]{:S(2)}) copy-start(bf16[2048,64]{0,1:T(8,128)(2,1)} %param.33) | copy-start | bytes 786436
  21.2 6.7 %copy-start.17 = (f32[3,64]{1,0:T(4,128)S(1)}, f32[3,64]{1,0:T(4,128)}, u32[]{:S(2)}) copy-start(f32[3,64]{1,0:T(4,128)} %param.36) | copy-start | bytes 2308
  21.2 6.7 %copy-start.18 = (f32[64]{0:T(128)S(1)}, f32[64]{0:T(128)}, u32[]{:S(2)}) copy-start(f32[64]{0:T(128)} %param.34) | copy-start | bytes 772
  21.2 7.6 %copy-start.8 = (bf16[4,6144]{1,0:T(4,128)(2,1)S(1)}, bf16[4,6144]{1,0:T(4,128)(2,1)}, u32[]{:S(2)}) copy-start(bf16[4,6144]{1,0:T(4,128)(2,1)} %param.38) | copy-start | bytes 147460
  21.2 7.7 %copy-start.14 = (f32[64]{0:T(128)S(1)}, f32[64]{0:T(128)}, u32[]{:S(2)}) copy-start(f32[64]{0:T(128)} %param.37) | copy-start | bytes 772
  21.5 7.6 %copy-start.9 = (f32[2048]{0:T(1024)S(1)}, f32[2048]{0:T(1024)}, u32[]{:S(2)}) copy-start(f32[2048]{0:T(1024)} %param.43) | copy-start | bytes 24580
  21.7 13.7 %copy-start.2 = (bf16[3,3,6144]{2,1,0:T(4,128)(2,1)S(1)}, bf16[3,3,6144]{2,1,0:T(4,128)(2,1)}, u32[]{:S(2)}) copy-start(bf16[3,3,6144]{2,1,0:T(4,128)(2,1)} %param.27) | copy-start | bytes 331780
  21.7 14.0 %copy-start.10 = (f32[6144]{0:T(1024)S(1)}, f32[6144]{0:T(1024)}, u32[]{:S(2)}) copy-start(f32[6144]{0:T(1024)} %param.39) | copy-start | bytes 73732
  24.4 10.6 %all-to-all-start.1 = ((bf16[16,3,640]{2,1,0:T(4,128)(2,1)}), bf16[16,3,640]{2,1,0:T(4,128)(2,1)S(1)}, u32[]{:S(2)}, u32[]{:S(2)}) async-start(bf16[16,3,640]{2,1,0:T(4,128)(2,1)} %reshape.143), calls=%async_computation.1 | async-start | bytes 163840 | tf_op jit(solution)/shard_map/all_to_all | solution.py:35
  38.0 20.9 %copy-start.11 = (f32[4096]{0:T(1024)S(1)}, f32[4096]{0:T(1024)}, u32[]{:S(2)}) copy-start(f32[4096]{0:T(1024)} %param.41) | copy-start | bytes 49156
  57.4 6.2 %copy-start.13 = (s32[3,6]{1,0:T(4,128)S(1)}, s32[3,6]{1,0:T(4,128)}, u32[]{:S(2)}) copy-start(s32[3,6]{1,0:T(4,128)} %param.45) | copy-start | bytes 220
  59.9 24.7 %copy-start.5 = (bf16[128,512]{1,0:T(8,128)(2,1)S(1)}, bf16[128,512]{1,0:T(8,128)(2,1)}, u32[]{:S(2)}) copy-start(bf16[128,512]{1,0:T(8,128)(2,1)} %param.50) | copy-start | bytes 393220
  59.9 17.9 %all-to-all-start.2 = ((bf16[16,3,4096]{2,1,0:T(4,128)(2,1)}), bf16[16,3,4096]{2,1,0:T(4,128)(2,1)S(1)}, u32[]{:S(2)}, u32[]{:S(2)}) async-start(bf16[16,3,4096]{2,1,0:T(4,128)(2,1)} %broadcast_in_dim.15), calls=%async_computation.2 | async-start | bytes 1048576 | tf_op jit(solution)/shard_map/all_to_all | solution.py:35
  78.2 6.5 %copy-start.6 = (bf16[128,512]{1,0:T(8,128)(2,1)S(1)}, bf16[128,512]{1,0:T(8,128)(2,1)}, u32[]{:S(2)}) copy-start(bf16[128,512]{1,0:T(8,128)(2,1)} %param.49) | copy-start | bytes 393220
  80.5 13.1 %all-to-all-start.3 = ((bf16[16,48,128]{2,1,0:T(8,128)(2,1)}), bf16[16,48,128]{2,1,0:T(8,128)(2,1)S(1)}, u32[]{:S(2)}, u32[]{:S(2)}) async-start(bf16[16,48,128]{2,1,0:T(8,128)(2,1)} %broadcast_in_dim.16), calls=%async_computation.3 | async-start | bytes 393216 | tf_op jit(solution)/shard_map/all_to_all | solution.py:35
  98.4 4.6 %copy-start.16 = (bf16[2048,16]{0,1:T(8,128)(2,1)S(1)}, bf16[2048,16]{0,1:T(8,128)(2,1)}, u32[]{:S(2)}) copy-start(bf16[2048,16]{0,1:T(8,128)(2,1)} %param.44) | copy-start | bytes 196612
  99.3 15.7 %all-to-all-start.4 = ((bf16[16,3,3072]{2,1,0:T(4,128)(2,1)}), bf16[16,3,3072]{2,1,0:T(4,128)(2,1)S(1)}, u32[]{:S(2)}, u32[]{:S(2)}) async-start(bf16[16,3,3072]{2,1,0:T(4,128)(2,1)} %reshape.150), calls=%async_computation.4 | async-start | bytes 786432 | tf_op jit(solution)/shard_map/all_to_all | solution.py:35

commit v2 on v1

--- a/solution.py
+++ b/solution.py
@@ -31,12 +31,60 @@
     return matmul(expert_hidden, weight_down).astype(jnp.bfloat16)
 
 
+def exchange_kernel(n, spread, source, landed, send_sem, recv_sem, own_sem):
+    me = lax.axis_index("ep")
+    barrier = pltpu.get_barrier_semaphore()
+    for step in range(1, n):
+        pl.semaphore_signal(
+            barrier, inc=1, device_id={"ep": lax.rem(me + step, n)}, device_id_type=pl.DeviceIdType.MESH
+        )
+    own = pltpu.make_async_copy(source if spread else source.at[me], landed.at[me], own_sem)
+    own.start()
+    pl.semaphore_wait(barrier, n - 1)
+    copies = []
+    for step in range(1, n):
+        target = lax.rem(me + step, n)
+        copy = pltpu.make_async_remote_copy(
+            src_ref=source if spread else source.at[target],
+            dst_ref=landed.at[me],
+            send_sem=send_sem.at[step],
+            recv_sem=recv_sem.at[step],
+            device_id={"ep": target},
+            device_id_type=pl.DeviceIdType.MESH,
+        )
+        copy.start()
+        copies.append(copy)
+    own.wait()
+    for copy in copies:
+        copy.wait()
+
+
+def send(source, shape, spread, ident):
+    n = shape[0]
+    return pl.pallas_call(
+        functools.partial(exchange_kernel, n, spread),
+        out_shape=jax.ShapeDtypeStruct(shape, source.dtype),
+        in_specs=[pl.BlockSpec(memory_space=pltpu.VMEM)],
+        out_specs=pl.BlockSpec(memory_space=pltpu.VMEM),
+        scratch_shapes=[
+            pltpu.SemaphoreType.DMA((n,)),
+            pltpu.SemaphoreType.DMA((n,)),
+            pltpu.SemaphoreType.DMA,
+        ],
+        compiler_params=pltpu.CompilerParams(collective_id=ident, has_side_effects=True),
+    )(source)
+
+
 def exchange(blocks, ident):
-    return lax.all_to_all(blocks, "ep", split_axis=0, concat_axis=0, tiled=True)
+    return send(blocks, blocks.shape, False, ident)
 
 
 def gather(block, ident):
-    return exchange(jnp.broadcast_to(block[None], (lax.axis_size("ep"),) + block.shape), ident)
+    return send(block, (lax.axis_size("ep"),) + block.shape, True, ident)
+
+
+def transposed(left, right):
+    return lax.dot_general(left, right, (((1,), (1,)), ((), ())), preferred_element_type=jnp.float32)
 
 
 def state_kernel(per_group, decay, inputs, write, read, carried, updated, mixed):
@@ -45,15 +93,29 @@
     scaled = inputs[0, 0]
     lane = lax.broadcasted_iota(jnp.int32, scaled.shape, 1)
     total = jnp.zeros(scaled.shape, jnp.float32)
-    for head in range(heads):
-        group = head // per_group
-        fresh = (
-            carried[0, head] * decay[row, part * heads + head]
-            + scaled[:, head : head + 1] * write[0, 0, group : group + 1]
-        )
-        updated[0, head] = fresh
-        column = jnp.sum(fresh * read[0, 0, group : group + 1], axis=1, keepdims=True)
-        total = jnp.where(lane == head, column, total)
+    entries = carried.shape[3]
+    head_dim = carried.shape[2]
+    for group in range(heads // per_group):
+        write_row = write[0, 0, group : group + 1]
+        spread = jnp.broadcast_to(read[0, 0, group : group + 1], (entries, entries))
+        spread_high = spread.astype(jnp.bfloat16)
+        spread_low = (spread - spread_high.astype(jnp.float32)).astype(jnp.bfloat16)
+        pieces = []
+        for head in range(group * per_group, (group + 1) * per_group):
+            fresh = (
+                carried[0, head] * decay[row, part * heads + head]
+                + scaled[:, head : head + 1] * write_row
+            )
+            updated[0, head] = fresh
+            pieces.append(fresh)
+        stacked = jnp.concatenate(pieces, axis=0)
+        high = stacked.astype(jnp.bfloat16)
+        low = (stacked - high.astype(jnp.float32)).astype(jnp.bfloat16)
+        columns = transposed(high, spread_high) + transposed(low, spread_high) + transposed(high, spread_low)
+        for place in range(per_group):
+            head = group * per_group + place
+            column = columns[place * head_dim : (place + 1) * head_dim, :heads]
+            total = jnp.where(lane == head, column, total)
     mixed[0, 0] = total
 
 

time: 119 us -> 109 us (0.916)
  Pallas kernels: 19.4 us -> 71.9 us
  waiting for transfers between devices: 47.8 us -> 0 us
  starting transfers between devices: 22.3 us -> 0 us
  other arithmetic: 4.91 us -> 10.1 us
  matrix products: 12.6 us -> 15.2 us
    pallas_call x0 -> x5, Pallas kernels: none -> 63.9 us  [send(): pl.pallas_call(functools.partial(exchange_kernel, n, spread), out_shape=j...]
    all_to_all x5 -> x0, waiting for transfers between devices: 47.8 us -> none  [exchange(): return lax.all_to_all(blocks, 'ep', split_axis=0, concat_axis=0, tiled=True)]
    all_to_all x5 -> x0, starting transfers between devices: 22.3 us -> none  [exchange(): return lax.all_to_all(blocks, 'ep', split_axis=0, concat_axis=0, tiled=True)]
    pallas_call x1, Pallas kernels: 19.4 us -> 8 us  [state_step(): pl.pallas_call(functools.partial(state_kernel, head_count // groups), gri...]
    broadcast_in_dim x3 -> x0, local copies, waits for them, and re-layouts: 3.39 us -> none  [gather(): jnp.broadcast_to(block[None], (lax.axis_size('ep'),) + block.shape)]
    dot_general x12, matrix products: 12.6 us -> 15.2 us  [matmul(): return jnp.dot(left, right, preferred_element_type=jnp.float32)]
    reduce_sum x4, other arithmetic: 1.32 us -> 2.54 us  [row_scale(): jnp.mean(values * values, axis=-1, keepdims=True) + epsilon]
  transfers between devices with their start and end apart: 5 -> 0, of which waited for: 5 -> 0; matrix products, arithmetic and copies ran while one was open for 4% -> 0% of each run, Pallas kernels for 0% -> 0%
where the time goes in v2:
time: 109 us; the launch traced here: 108 us
  Pallas kernels  71.9 us (66%)
  matrix products  15.2 us (14%)
  other arithmetic  10.1 us (9%)
  local copies, waits for them, and re-layouts  9.48 us (9%)
    pallas_call x5, Pallas kernels, send(): pl.pallas_call(functools.partial(exchange_kernel, n, spread), out_shape=j...  63.9 us
    dot_general x12, matrix products, matmul(): return jnp.dot(left, right, preferred_element_type=jnp.float32)  15.2 us
    pallas_call x1, Pallas kernels, state_step(): pl.pallas_call(functools.partial(state_kernel, head_count // groups), gri...  8 us
    reduce_sum x4, other arithmetic, row_scale(): jnp.mean(values * values, axis=-1, keepdims=True) + epsilon  2.54 us

profile of v2, /device:TPU:0, one launch (start us, length us, event | category | flops | bytes accessed | tf_op | source)
XLA Modules:
  0.0 107.7 jit_solution(9910501801766522415)
XLA Ops:
  0.7 12.7 %shard_map.265 = bf16[16,3,2048]{2,1,0:T(4,128)(2,1)} custom-call(bf16[3,2048]{1,0:T(4,128)(2,1)} %source.1), custom_call_target="tpu_custom_call" | custom-call | tf_op jit(solution)/shard_map/pallas_call | solution.py:64
  13.4 1.1 %reshape.148 = f32[48,2048]{1,0:T(8,128)S(1)} reshape(bf16[16,3,2048]{2,1,0:T(4,128)(2,1)} %shard_map.265) | data formatting | bytes 589824 | tf_op jit(solution)/shard_map/convert_element_type | solution.py:183
  14.5 1.2 %multiply_reduce_fusion = f32[16,3]{1,0:T(8,128)S(1)} fusion(bf16[16,3,2048]{2,1,0:T(4,128)(2,1)} %shard_map.265), kind=kLoop, calls=%fused_computation.29 | loop fusion | flops 294864 | bytes 196800 | tf_op jit(solution)/shard_map/reduce_sum | solution.py:20
  15.7 0.9 multiply_convert_fusion
  16.6 1.2 %convolution_convert_fusion.5 = bf16[48,64]{1,0:T(8,128)(2,1)S(1)} fusion(bf16[48,2048]{1,0:T(8,128)(2,1)S(1)} %multiply_convert_fusion, bf16[2048,64]{0,1:T(8,128)(2,1)} %param.32), kind=kOutput, calls=%fused_computation.16 | convolution fusion | flops 12585984 | bytes 464896 | tf_op jit(solution)/shard_map/dot_general | solution.py:24
  17.8 1.2 %convolution_convert_fusion.6 = bf16[48,64]{1,0:T(8,128)(2,1)S(1)} fusion(bf16[48,2048]{1,0:T(8,128)(2,1)S(1)} %multiply_convert_fusion, bf16[2048,64]{0,1:T(8,128)(2,1)} %param.31), kind=kOutput, calls=%fused_computation.17 | convolution fusion | flops 12585984 | bytes 464896 | tf_op jit(solution)/shard_map/dot_general | solution.py:24
  20.4 10.0 %shard_map.266 = bf16[16,3,640]{2,1,0:T(4,128)(2,1)} custom-call(bf16[16,3,640]{2,1,0:T(4,128)(2,1)} %reshape.140.source), custom_call_target="tpu_custom_call" | custom-call | tf_op jit(solution)/shard_map/pallas_call | solution.py:64
  32.0 1.8 %subtract_exponential_fusion = (f32[3,64]{1,0:T(4,128)}, f32[3,64]{1,0:T(4,128)S(1)}) fusion(f32[3,64]{1,0:T(4,128)} %param.36, f32[64]{0:T(128)S(1)} %exp.32, f32[64]{0:T(128)} %param.34, bf16[2048,64]{0,1:T(8,128)(2,1)} %param.33, bf16[3,2048]{1,0:T(4,128)(2,1)S(1)} %copy-done.8, f32[2048]{0:T(1024)} %param.40, f32[3]{0:T(128)S(1)} %add_rsqrt_fusion.3), kind=kOutput, calls=%fused_computation.89 | convolution fusion | flops 812736 | bytes 285452 | tf_op jit(solution)/shard_map/dot_general | solution.py:24
  33.8 0.9 slice_bitcast_fusion.1
  38.5 8.0 %shard_map.267 = (f32[3,64,64,128]{3,2,1,0:T(8,128)}, f32[3,2,64,32]{3,2,1,0:T(8,128)}) custom-call(f32[3,64]{1,0:T(4,128)} %get-tuple-element.15.decay, f32[3,2,64,32]{3,2,1,0:T(8,128)} %multiply_bitcast_fusion.inputs, f32[3,2,4,128]{3,2,1,0:T(4,128)} %reshape_reshape.6.write, f32[3,2,4,128]{3,2,1,0:T(4,128)} %reshape_reshape.7.read, f32[3,64,64,128]{3,2,1,0:T(8,128)} %carried.1), custom_call_target="tpu_custom_call" | custom-call | tf_op jit(solution)/shard_map/pallas_call | solution.py:131
  46.5 1.1 copy.44
  48.8 15.1 %shard_map.268 = bf16[16,3,4096]{2,1,0:T(4,128)(2,1)} custom-call(bf16[3,4096]{1,0:T(4,128)(2,1)} %multiply_convert_fusion.1.source), custom_call_target="tpu_custom_call" | custom-call | tf_op jit(solution)/shard_map/pallas_call | solution.py:64
  63.9 1.4 %reshape.146 = bf16[48,4096]{1,0:T(8,128)(2,1)S(1)} reshape(bf16[16,3,4096]{2,1,0:T(4,128)(2,1)} %shard_map.268) | data formatting | bytes 786432 | tf_op jit(solution)/shard_map/reshape | solution.py:226
  65.3 1.5 %fusion.14.source = bf16[48,128]{1,0:T(8,128)(2,1)S(1)} fusion(bf16[48,4096]{1,0:T(8,128)(2,1)S(1)} %reshape.146, bf16[4096,128]{1,0:T(8,128)(2,1)} %param.42, f32[48,2048]{1,0:T(8,128)S(1)} %reshape.148, s32[]{:T(128)S(6)} %select_n.20), kind=kOutput, calls=%fused_computation.15 | convolution fusion | flops 50343936 | bytes 1478660 | tf_op jit(solution)/shard_map/dot_general | solution.py:24
  67.4 12.1 %shard_map.269 = bf16[16,48,128]{2,1,0:T(8,128)(2,1)} custom-call(bf16[48,128]{1,0:T(8,128)(2,1)} %copy-done.5), custom_call_target="tpu_custom_call" | custom-call | tf_op jit(solution)/shard_map/pallas_call | solution.py:64
  79.5 1.1 %fusion.20 = f32[48]{0:T(128)S(1)} fusion(bf16[16,48,128]{2,1,0:T(8,128)(2,1)} %shard_map.269), kind=kLoop, calls=%fused_computation.30 | loop fusion | flops 294864 | bytes 196800 | tf_op jit(solution)/shard_map/reduce_sum | solution.py:20
  80.7 2.2 %fusion.4 = f32[48,512]{1,0:T(8,128)S(1)} fusion(bf16[1,2048,512]{2,1,0:T(8,128)(2,1)} %param.46, bf16[16,48,128]{2,1,0:T(8,128)(2,1)} %shard_map.269, f32[16,128]{1,0:T(8,128)S(1)} %bitcast.81, f32[48]{0:T(128)S(1)} %add_rsqrt_fusion.2), kind=kOutput, calls=%fused_computation.6 | convolution fusion | flops 101056512 | bytes 2400448 | tf_op jit(solution)/shard_map/dot_general | solution.py:24
  82.9 2.5 %convolution_convert_fusion = bf16[48,2048]{1,0:T(8,128)(2,1)S(1)} fusion(bf16[1,512,2048]{2,1,0:T(8,128)(2,1)S(1)} %copy-done, bf16[1,2048,512]{2,1,0:T(8,128)(2,1)} %param.47, f32[48,512]{1,0:T(8,128)S(1)} %fusion.4, bf16[16,48,128]{2,1,0:T(8,128)(2,1)S(1)} %copy-done.1, f32[16,128]{1,0:T(8,128)S(1)} %bitcast.82, f32[48]{0:T(128)S(1)} %add_rsqrt_fusion.2), kind=kOutput, calls=%fused_computation | convolution fusion | flops 201965568 | bytes 4694208 | tf_op jit(solution)/shard_map/dot_general | solution.py:24
  85.5 0.9 reshape.147.source
  86.4 14.1 %shard_map.270 = bf16[16,3,3072]{2,1,0:T(4,128)(2,1)} custom-call(bf16[16,3,3072]{2,1,0:T(4,128)(2,1)} %reshape.147.source), custom_call_target="tpu_custom_call" | custom-call | tf_op jit(solution)/shard_map/pallas_call | solution.py:64
  100.6 1.1 convert_element_type.129
  102.6 1.2 %fusion.61 = (f32[3]{0:T(128)S(1)}, f32[3,16]{1,0:T(4,128)S(1)}) fusion(pred[3,16]{1,0:T(4,128)(4,1)S(1)} %fusion.46, bf16[2048,16]{0,1:T(8,128)(2,1)S(1)} %copy-done.14, f32[48,2048]{1,0:T(8,128)} %copy_bitcast_fusion, s32[]{:T(128)S(6)} %select_n.22, f32[2048]{0:T(1024)S(1)} %copy-done.9, f32[3]{0:T(128)S(1)} %dynamic-slice.4), kind=kOutput, calls=%fused_computation.98 | convolution fusion | flops 215277 | bytes 106764 | tf_op jit(solution)/shard_map/dot_general | solution.py:24
  104.2 2.6 %fusion = bf16[3,2048]{1,0:T(4,128)(2,1)} fusion(bf16[512,2048]{1,0:T(8,128)(2,1)} %param.51, f32[3,2048]{1,0:T(4,128)S(1)} %fusion.19, f32[48,2048]{1,0:T(8,128)} %copy_bitcast_fusion, s32[]{:T(128)S(6)} %select_n.22, f32[3,1024]{1,0:T(4,128)S(1)} %slice_reduce_fusion, f32[3]{0:T(128)S(1)} %dynamic-slice.4), kind=kOutput, calls=%fused_computation.2 | convolution fusion | flops 6322176 | bytes 2170896 | tf_op jit(solution)/shard_map/dot_general | solution.py:24
  106.8 0.9 fusion.30
  (78 shorter events, 10.0 us)
Async XLA Ops:
  0.6 82.3 %copy-start = (bf16[1,512,2048]{2,1,0:T(8,128)(2,1)S(1)}, bf16[1,512,2048]{2,1,0:T(8,128)(2,1)}, u32[]{:S(2)}) copy-start(bf16[1,512,2048]{2,1,0:T(8,128)(2,1)} %param.48) | copy-start | bytes 6291460
  0.6 18.4 %copy-start.2 = (bf16[2048,256]{1,0:T(8,128)(2,1)S(1)}, bf16[2048,256]{1,0:T(8,128)(2,1)}, u32[]{:S(2)}) copy-start(bf16[2048,256]{1,0:T(8,128)(2,1)} %param.30) | copy-start | bytes 3145732
  15.7 3.6 %copy-start.3 = (bf16[2048,256]{1,0:T(8,128)(2,1)S(1)}, bf16[2048,256]{1,0:T(8,128)(2,1)}, u32[]{:S(2)}) copy-start(bf16[2048,256]{1,0:T(8,128)(2,1)} %param.29) | copy-start | bytes 3145732
  16.6 15.2 %copy-start.8 = (bf16[3,2048]{1,0:T(4,128)(2,1)S(1)}, bf16[3,2048]{1,0:T(4,128)(2,1)}, u32[]{:S(2)}) copy-start(bf16[3,2048]{1,0:T(4,128)(2,1)} %source.1) | copy-start | bytes 36868
  19.3 16.4 %copy-start.4 = (bf16[3,3,6144]{2,1,0:T(4,128)(2,1)S(1)}, bf16[3,3,6144]{2,1,0:T(4,128)(2,1)}, u32[]{:S(2)}) copy-start(bf16[3,3,6144]{2,1,0:T(4,128)(2,1)} %param.27) | copy-start | bytes 331780
  19.3 16.8 %copy-start.10 = (f32[6144]{0:T(1024)S(1)}, f32[6144]{0:T(1024)}, u32[]{:S(2)}) copy-start(f32[6144]{0:T(1024)} %param.39) | copy-start | bytes 73732
  38.5 9.2 %copy-start.13 = (f32[64]{0:T(128)S(1)}, f32[64]{0:T(128)}, u32[]{:S(2)}) copy-start(f32[64]{0:T(128)} %param.37) | copy-start | bytes 772
  38.5 9.7 %copy-start.11 = (f32[4096]{0:T(1024)S(1)}, f32[4096]{0:T(1024)}, u32[]{:S(2)}) copy-start(f32[4096]{0:T(1024)} %param.41) | copy-start | bytes 49156
  46.5 20.3 %copy-start.9 = (f32[2048]{0:T(1024)S(1)}, f32[2048]{0:T(1024)}, u32[]{:S(2)}) copy-start(f32[2048]{0:T(1024)} %param.43) | copy-start | bytes 24580
  46.5 20.4 %copy-start.6 = (bf16[128,512]{1,0:T(8,128)(2,1)S(1)}, bf16[128,512]{1,0:T(8,128)(2,1)}, u32[]{:S(2)}) copy-start(bf16[128,512]{1,0:T(8,128)(2,1)} %param.50) | copy-start | bytes 393220
  47.6 19.5 %copy-start.7 = (bf16[128,512]{1,0:T(8,128)(2,1)S(1)}, bf16[128,512]{1,0:T(8,128)(2,1)}, u32[]{:S(2)}) copy-start(bf16[128,512]{1,0:T(8,128)(2,1)} %param.49) | copy-start | bytes 393220
  66.8 0.6 copy-start.5
  79.5 3.4 %copy-start.1 = (bf16[16,48,128]{2,1,0:T(8,128)(2,1)S(1)}, bf16[16,48,128]{2,1,0:T(8,128)(2,1)}, u32[]{:S(2)}) copy-start(bf16[16,48,128]{2,1,0:T(8,128)(2,1)} %shard_map.269) | copy-start | bytes 589828
  85.5 16.2 %copy-start.12 = (s32[3,6]{1,0:T(4,128)S(1)}, s32[3,6]{1,0:T(4,128)}, u32[]{:S(2)}) copy-start(s32[3,6]{1,0:T(4,128)} %param.45) | copy-start | bytes 220
  85.5 17.1 %copy-start.14 = (bf16[2048,16]{0,1:T(8,128)(2,1)S(1)}, bf16[2048,16]{0,1:T(8,128)(2,1)}, u32[]{:S(2)}) copy-start(bf16[2048,16]{0,1:T(8,128)(2,1)} %param.44) | copy-start | bytes 196612
